TPU v7x, 32 devices: a whole 2x2x4 slice. The times are simulated.
32 devices in a mesh: ep: 8 (over z, core), tp: 4 (over y, x).
Axes of the slice: x: 2, y: 2, z: 4, core: 2. Of those that a mesh axis runs over, the one named last changes fastest.
Arguments:
- tokens: bfloat16 [2048, 2048], P('ep'), may hold values from -6 to 6
- norm_gain: float32 [2048], replicated, may hold values from 0.1 to 1.9
- route_ids: int32 [2048, 4], P('ep'), may hold values from 0 to 15, all different within a row; in each aligned block of 256 rows (0 to 255, 256 to 511, ...) at most 96 rows name the same one
- route_weights: float32 [2048, 4], P('ep'), may hold values from 0.1 to 1
- w_gate: bfloat16 [16, 2048, 2048], P('ep', None, 'tp'), may hold values from -0.33007812 to 0.33007812
- w_up: bfloat16 [16, 2048, 2048], P('ep', None, 'tp'), may hold values from -0.33007812 to 0.33007812
- w_down: bfloat16 [16, 2048, 2048], P('ep', None, 'tp'), may hold values from -0.026489258 to 0.026489258
Outputs:
- mixed_out: bfloat16 [2048, 2048], P('ep', 'tp')
Inputs may be any that keep to these rules, and one draw needn't show every extreme that they name: `route_ids`: each token names 4 different experts. Within the tokens of one index of ep (aligned blocks of 256 tokens) no expert is named more than 96 times, a bound that some block reaches.
All inputs are finite; a program needn't handle non-finite values.
Results may differ from a plain program's by a relative error of at most 0.007.
Values may be sent and summed in bfloat16 or wider, within the bound.
A program may use at most 64 MiB of HBM per device.

v0:
```python
import jax
import jax.numpy as jnp
from jax import lax
from jax.sharding import PartitionSpec as P

swiglu_limit = 7.0
swiglu_alpha = 1.702
norm_eps = 1e-05


def clamped_units(gate_pre, up_pre):
    capped = jnp.minimum(gate_pre, swiglu_limit)
    linear = jnp.clip(up_pre, -swiglu_limit, swiglu_limit)
    return capped * jax.nn.sigmoid(swiglu_alpha * capped) * (linear + 1.0)


def expert_work(outgoing, gate_weight, up_weight, down_weight):
    received = lax.all_to_all(outgoing, "ep", split_axis=1, concat_axis=1, tiled=True)
    local_count, sources, capacity, columns = received.shape
    row_count = sources * capacity
    row_block = received.reshape(local_count, row_count, columns)
    shard_piece = lax.all_gather(row_block, "tp", axis=2, tiled=True)
    gate_sum = jnp.einsum(
        "lrd,ldf->lrf", shard_piece, gate_weight, preferred_element_type=jnp.float32
    )
    up_sum = jnp.einsum("lrd,ldf->lrf", shard_piece, up_weight, preferred_element_type=jnp.float32)
    activation = clamped_units(gate_sum, up_sum).astype(jnp.bfloat16)
    out_cols = down_weight.shape[2]
    result = jnp.einsum(
        "lrf,lfd->lrd",
        lax.all_gather(activation, "tp", axis=2, tiled=True),
        down_weight,
        preferred_element_type=jnp.float32,
    )
    result = result.astype(jnp.bfloat16).reshape(local_count, sources, capacity, out_cols)
    return lax.all_to_all(result, "ep", split_axis=1, concat_axis=1, tiled=True)


def per_device(tokens, norm_gain, route_ids, route_weights, w_gate, w_up, w_down):
    local_count = w_gate.shape[0]
    sources = lax.axis_size("ep")
    tp_count = lax.axis_size("tp")
    width = tokens.shape[1]
    columns = width // tp_count
    experts = local_count * sources
    tok_rows, top_count = route_ids.shape
    capacity = 3 * tok_rows * top_count // (2 * experts)
    values = tokens.astype(jnp.float32)
    row_mean = jnp.mean(values, axis=1, keepdims=True)
    centred = values - row_mean
    row_var = jnp.mean(centred * centred, axis=1, keepdims=True)
    offset = lax.axis_index("tp") * columns
    own_cols = lax.dynamic_slice_in_dim(centred, offset, columns, 1)
    own_gain = lax.dynamic_slice_in_dim(norm_gain, offset, columns, 0)
    normed = (own_cols * lax.rsqrt(row_var + norm_eps) * own_gain).astype(jnp.bfloat16)
    flat_ids = route_ids.reshape(-1)
    matches = (flat_ids[:, None] == jnp.arange(experts, dtype=jnp.int32)[None, :]).astype(jnp.int32)
    earlier = jnp.cumsum(matches, axis=0) - matches
    slot_index = jnp.sum(earlier * matches, axis=1)
    position = (
        flat_ids % local_count * (sources * capacity)
        + flat_ids // local_count * capacity
        + slot_index
    )
    buffer_rows = local_count * sources * capacity
    placed = (
        position.reshape(tok_rows, top_count)[:, :, None]
        == jnp.arange(buffer_rows, dtype=jnp.int32)[None, None, :]
    )
    placement_matrix = jnp.any(placed, axis=1).astype(jnp.bfloat16)
    outgoing = jnp.einsum("tp,td->pd", placement_matrix, normed, preferred_element_type=jnp.float32)
    outgoing = outgoing.astype(jnp.bfloat16).reshape(local_count, sources, capacity, columns)
    returned = jnp.concatenate(
        [
            expert_work(
                outgoing[number : number + 1],
                w_gate[number : number + 1],
                w_up[number : number + 1],
                w_down[number : number + 1],
            )
            for number in range(local_count)
        ],
        axis=0,
    )
    flat_out = returned.reshape(buffer_rows, columns)
    picked = flat_out[position].reshape(tok_rows, top_count, columns).astype(jnp.float32)
    return jnp.sum(picked * route_weights[:, :, None], axis=1).astype(jnp.bfloat16)


def solution(mesh):
    return jax.shard_map(
        per_device,
        mesh=mesh,
        in_specs=(
            P("ep", None),
            P(),
            P("ep", None),
            P("ep", None),
            P("ep", None, "tp"),
            P("ep", None, "tp"),
            P("ep", None, "tp"),
        ),
        out_specs=P("ep", "tp"),
        check_vma=False,
    )
```

profile of v0, /device:TPU:0, one launch (start us, length us, event | category | flops | bytes accessed | tf_op | source)
XLA Modules:
  0.0 269.5 jit_solution(14024327743090888040)
XLA Ops:
  6.5 0.0 copy-start
  6.5 0.0 all-gather.7.cloned.1.call-start
  6.5 0.9 copy.62
  7.4 0.1 eq.44
  7.6 0.1 eq.40
  7.7 4.5 %reduce-window.6 = s32[16,8,128]{2,1,0:T(8,128)S(1)} reduce-window(s32[16,8,128]{2,1,0:T(8,128)S(1)} %fusion.42, s32[]{:T(128)} %constant.28.clone.1), window={size=1x1x128 pad=0_0x0_0x127_0}, to_apply=%region_0.0 | reduce-window | flops 2080768 | bytes 131076 | tf_op jit(solution)/shard_map/reduce-window
  12.2 0.1 slice.50
  12.3 0.1 copy.64
  12.5 0.1 copy.65
  12.5 0.1 broadcast_add_fusion
  12.7 0.1 reduce_sum.41
  12.8 0.1 copy.66
  12.9 0.7 fusion.45
  13.6 1.7 fusion
  15.3 0.0 copy-done
  15.3 0.2 convert_reduce_fusion
  15.6 0.4 multiply_reduce_fusion.1
  16.0 0.8 dynamic_slice.7
  16.8 1.7 convolution_convert_fusion
  18.5 0.1 fusion.53
  18.6 27.2 %all_to_all.20 = bf16[1,8,96,512]{3,2,0,1:T(8,128)(2,1)} all-to-all(bf16[1,8,96,512]{3,2,0,1:T(8,128)(2,1)S(1)} %bitcast.82), channel_id=1, replica_groups=mesh['ep'=8,'tp'=4] {'ep'}, dimensions={1} | all-to-all | bytes 1572864 | tf_op jit(solution)/shard_map/all_to_all | solution.py:18
  45.8 0.0 all-gather.7.cloned.1.call-update
  45.8 0.0 all-gather.9.cloned.1.call-start
  45.9 24.0 %all_to_all.21 = bf16[1,8,96,512]{3,2,0,1:T(8,128)(2,1)} all-to-all(bf16[1,8,96,512]{3,2,0,1:T(8,128)(2,1)S(1)} %bitcast.81), channel_id=1, replica_groups=mesh['ep'=8,'tp'=4] {'ep'}, dimensions={1} | all-to-all | bytes 1572864 | tf_op jit(solution)/shard_map/all_to_all | solution.py:18
  69.9 0.0 all-gather.9.cloned.1.call-update
  69.9 0.0 all-gather.11.cloned.1.call-start
  70.0 18.6 %all-gather.7.cloned.1.call-done = bf16[1,768,2048]{2,1,0:T(8,128)(2,1)} async-done(((bf16[1,768,512]{2,1,0:T(8,128)(2,1)}), bf16[1,768,2048]{2,1,0:T(8,128)(2,1)}) %all-gather.7.cloned.1.call-update) | async-done | bytes 3145744 | tf_op jit(solution)/shard_map/all_gather | solution.py:22
  88.6 0.0 copy-start.2
  88.6 0.0 copy-start.5
  88.6 4.5 %fusion.7 = f32[768,512]{1,0:T(8,128)S(1)} fusion(bf16[1,768,2048]{2,1,0:T(8,128)(2,1)} %all-gather.7.cloned.1.call-done, bf16[2,2048,512]{2,1,0:T(8,128)(2,1)} %param.11), kind=kOutput, calls=%fused_computation.9 | convolution fusion | flops 1610612736 | bytes 6815744 | tf_op jit(solution)/shard_map/lrd,ldf->lrf/dot_general | solution.py:23
  93.1 0.0 copy-done.2
  93.1 0.2 copy-done.5
  93.3 3.0 %multiply_convert_fusion.1 = bf16[768,512]{1,0:T(8,128)(2,1)} fusion(f32[768,512]{1,0:T(8,128)S(1)} %fusion.7, bf16[2,2048,512]{2,1,0:T(8,128)(2,1)S(1)} %copy-done.2, bf16[1,768,2048]{2,1,0:T(8,128)(2,1)S(1)} %copy-done.5), kind=kOutput, calls=%fused_computation.32 | convolution fusion | flops 1614544896 | bytes 7602176 | tf_op jit(solution)/shard_map/lrd,ldf->lrf/dot_general | solution.py:26
  96.3 0.0 all-gather.11.cloned.1.call-update
  96.4 0.0 all-gather.13.cloned.1.call-start
  96.4 37.8 %all-gather.9.cloned.1.call-done = bf16[1,768,2048]{2,1,0:T(8,128)(2,1)} async-done(((bf16[1,768,512]{2,1,0:T(8,128)(2,1)}), bf16[1,768,2048]{2,1,0:T(8,128)(2,1)}) %all-gather.9.cloned.1.call-update) | async-done | bytes 3145744 | tf_op jit(solution)/shard_map/all_gather | solution.py:22
  134.2 0.0 copy-start.3
  134.2 0.0 copy-start.4
  134.2 4.5 %fusion.3 = f32[768,512]{1,0:T(8,128)S(1)} fusion(bf16[1,768,2048]{2,1,0:T(8,128)(2,1)} %all-gather.9.cloned.1.call-done, bf16[2,2048,512]{2,1,0:T(8,128)(2,1)} %param.11), kind=kOutput, calls=%fused_computation.5 | convolution fusion | flops 1610612736 | bytes 6815744 | tf_op jit(solution)/shard_map/lrd,ldf->lrf/dot_general | solution.py:23
  138.7 0.0 copy-done.3
  138.7 0.2 copy-done.4
  138.9 3.0 %multiply_convert_fusion = bf16[768,512]{1,0:T(8,128)(2,1)} fusion(f32[768,512]{1,0:T(8,128)S(1)} %fusion.3, bf16[2,2048,512]{2,1,0:T(8,128)(2,1)S(1)} %copy-done.3, bf16[1,768,2048]{2,1,0:T(8,128)(2,1)S(1)} %copy-done.4), kind=kOutput, calls=%fused_computation.31 | convolution fusion | flops 1614544896 | bytes 7602176 | tf_op jit(solution)/shard_map/lrd,ldf->lrf/dot_general | solution.py:26
  141.9 0.0 all-gather.13.cloned.1.call-update
  141.9 37.8 %all-gather.11.cloned.1.call-done = bf16[768,2048]{1,0:T(8,128)(2,1)} async-done(((bf16[768,512]{1,0:T(8,128)(2,1)}), bf16[768,2048]{1,0:T(8,128)(2,1)}) %all-gather.11.cloned.1.call-update) | async-done | bytes 3145744 | tf_op jit(solution)/shard_map/all_gather | solution.py:31
  179.8 5.2 %fusion.31 = bf16[768,512]{1,0:T(8,128)(2,1)} fusion(bf16[768,2048]{1,0:T(8,128)(2,1)} %all-gather.11.cloned.1.call-done, bf16[2,2048,512]{2,1,0:T(8,128)(2,1)} %param.13), kind=kOutput, calls=%fused_computation.33 | convolution fusion | flops 1611005952 | bytes 6029312 | tf_op jit(solution)/shard_map/lrf,lfd->lrd/dot_general | solution.py:29
  185.0 4.6 %all-to-all-start.1 = ((bf16[1,8,96,512]{3,2,0,1:T(8,128)(2,1)}), bf16[1,8,96,512]{3,2,0,1:T(8,128)(2,1)S(1)}, u32[]{:S(2)}, u32[]{:S(2)}) async-start(bf16[1,8,96,512]{3,2,0,1:T(8,128)(2,1)} %bitcast.10), calls=%async_computation.1 | async-start | bytes 1572864 | tf_op jit(solution)/shard_map/all_to_all | solution.py:36
  189.6 0.0 copy-start.1
  189.6 35.6 %all-gather.13.cloned.1.call-done = bf16[768,2048]{1,0:T(8,128)(2,1)} async-done(((bf16[768,512]{1,0:T(8,128)(2,1)}), bf16[768,2048]{1,0:T(8,128)(2,1)}) %all-gather.13.cloned.1.call-update) | async-done | bytes 3145744 | tf_op jit(solution)/shard_map/all_gather | solution.py:31
  225.2 5.2 %fusion.34 = bf16[768,512]{1,0:T(8,128)(2,1)} fusion(bf16[768,2048]{1,0:T(8,128)(2,1)} %all-gather.13.cloned.1.call-done, bf16[2,2048,512]{2,1,0:T(8,128)(2,1)} %param.13), kind=kOutput, calls=%fused_computation.34 | convolution fusion | flops 1611005952 | bytes 6029312 | tf_op jit(solution)/shard_map/lrf,lfd->lrd/dot_general | solution.py:29
  230.4 0.0 all-to-all-done.1
  230.4 4.6 %all-to-all-start.3 = ((bf16[1,8,96,512]{3,2,0,1:T(8,128)(2,1)}), bf16[1,8,96,512]{3,2,0,1:T(8,128)(2,1)S(1)}, u32[]{:S(2)}, u32[]{:S(2)}) async-start(bf16[1,8,96,512]{3,2,0,1:T(8,128)(2,1)} %bitcast.19), calls=%async_computation.3 | async-start | bytes 1572864 | tf_op jit(solution)/shard_map/all_to_all | solution.py:36
  235.0 0.1 reshape.289
  235.1 0.0 copy-done.1
  235.1 0.1 copy.73
  235.3 20.6 %all-to-all-done.3 = bf16[1,8,96,512]{3,2,0,1:T(8,128)(2,1)S(1)} async-done(((bf16[1,8,96,512]{3,2,0,1:T(8,128)(2,1)}), bf16[1,8,96,512]{3,2,0,1:T(8,128)(2,1)S(1)}, u32[]{:S(2)}, u32[]{:S(2)}) %all-to-all-start.3) | async-done | bytes 786464 | tf_op jit(solution)/shard_map/all_to_all | solution.py:36
  255.9 0.1 pad_maximum_fusion
  256.1 0.1 copy.71
  256.2 4.0 %gather_fusion = bf16[1024,512]{1,0:T(8,128)(2,1)S(1)} fusion(bf16[1536,512]{1,0:T(8,128)(2,1)S(1)} %bitcast.78, s32[1024]{0:T(1024)S(1)} %broadcast_clamp_fusion), kind=kCustom, calls=%fused_computation | custom fusion | bytes 2101248 | tf_op jit(solution)/shard_map/gather | solution.py:86
  260.2 0.7 reshape.290
  260.9 2.1 multiply_reduce_fusion
  (8 shorter events, 0.1 us)
Async XLA Ops:
  6.5 8.8 %copy-start = (bf16[256,2048]{1,0:T(8,128)(2,1)S(1)}, bf16[256,2048]{1,0:T(8,128)(2,1)}, u32[]{:S(2)}) copy-start(bf16[256,2048]{1,0:T(8,128)(2,1)} %param.7) | copy-start | bytes 3145732
  6.5 82.1 %all-gather.7.cloned.1.call-start = ((), (), s32[]{:S(2)}) async-start(), calls=%async_computation.4 | async-start | bytes 3932160 | tf_op jit(solution)/shard_map/all_gather | solution.py:22
  45.8 88.4 %all-gather.9.cloned.1.call-start = ((), (), s32[]{:S(2)}) async-start(), calls=%async_computation.5 | async-start | bytes 3932160 | tf_op jit(solution)/shard_map/all_gather | solution.py:22
  69.9 109.8 %all-gather.11.cloned.1.call-start = ((), (), s32[]{:S(2)}) async-start(), calls=%async_computation.6 | async-start | bytes 3932160 | tf_op jit(solution)/shard_map/all_gather | solution.py:31
  88.6 4.5 %copy-start.2 = (bf16[2,2048,512]{2,1,0:T(8,128)(2,1)S(1)}, bf16[2,2048,512]{2,1,0:T(8,128)(2,1)}, u32[]{:S(2)}) copy-start(bf16[2,2048,512]{2,1,0:T(8,128)(2,1)} %param.12) | copy-start | bytes 12582916
  88.6 4.7 %copy-start.5 = (bf16[1,768,2048]{2,1,0:T(8,128)(2,1)S(1)}, bf16[1,768,2048]{2,1,0:T(8,128)(2,1)}, u32[]{:S(2)}) copy-start(bf16[1,768,2048]{2,1,0:T(8,128)(2,1)} %all-gather.7.cloned.1.call-done) | copy-start | bytes 9437188
  96.4 128.8 %all-gather.13.cloned.1.call-start = ((), (), s32[]{:S(2)}) async-start(), calls=%async_computation.7 | async-start | bytes 3932160 | tf_op jit(solution)/shard_map/all_gather | solution.py:31
  134.2 4.5 %copy-start.3 = (bf16[2,2048,512]{2,1,0:T(8,128)(2,1)S(1)}, bf16[2,2048,512]{2,1,0:T(8,128)(2,1)}, u32[]{:S(2)}) copy-start(bf16[2,2048,512]{2,1,0:T(8,128)(2,1)} %param.12) | copy-start | bytes 12582916
  134.2 4.7 %copy-start.4 = (bf16[1,768,2048]{2,1,0:T(8,128)(2,1)S(1)}, bf16[1,768,2048]{2,1,0:T(8,128)(2,1)}, u32[]{:S(2)}) copy-start(bf16[1,768,2048]{2,1,0:T(8,128)(2,1)} %all-gather.9.cloned.1.call-done) | copy-start | bytes 9437188
  185.0 45.4 %all-to-all-start.1 = ((bf16[1,8,96,512]{3,2,0,1:T(8,128)(2,1)}), bf16[1,8,96,512]{3,2,0,1:T(8,128)(2,1)S(1)}, u32[]{:S(2)}, u32[]{:S(2)}) async-start(bf16[1,8,96,512]{3,2,0,1:T(8,128)(2,1)} %bitcast.10), calls=%async_computation.1 | async-start | bytes 1572864 | tf_op jit(solution)/shard_map/all_to_all | solution.py:36
  189.6 45.5 %copy-start.1 = (f32[256,4]{0,1:T(4,128)S(1)}, f32[256,4]{0,1:T(4,128)}, u32[]{:S(2)}) copy-start(f32[256,4]{0,1:T(4,128)} %param.10) | copy-start | bytes 12292
  230.4 25.6 %all-to-all-start.3 = ((bf16[1,8,96,512]{3,2,0,1:T(8,128)(2,1)}), bf16[1,8,96,512]{3,2,0,1:T(8,128)(2,1)S(1)}, u32[]{:S(2)}, u32[]{:S(2)}) async-start(bf16[1,8,96,512]{3,2,0,1:T(8,128)(2,1)} %bitcast.19), calls=%async_computation.3 | async-start | bytes 1572864 | tf_op jit(solution)/shard_map/all_to_all | solution.py:36
Sparse Core Ops, SparseCore 0:
  45.9 42.6 all-gather.6
  90.4 43.6 all-gather.8
  136.0 43.6 all-gather.10
  181.4 43.6 all-gather.12
where the time goes:
time: 270 us; the launch traced here: 269 us
  waiting for transfers between devices  150 us (56%)
  blocking collectives  51.2 us (19%)
  matrix products  27 us (10%)
  between operations  13.3 us (5%)
  other arithmetic  10 us (4%)
  starting transfers between devices  9.36 us (3%)
  local copies, waits for them, and re-layouts  8.03 us (3%)
    all_gather x2, waiting for transfers between devices, expert_work(): lax.all_gather(activation, 'tp', axis=2, tiled=True)  73.4 us
    all_gather x2, waiting for transfers between devices, expert_work(): shard_piece = lax.all_gather(row_block, 'tp', axis=2, tiled=True)  56.4 us
    all_to_all x2, blocking collectives, expert_work(): lax.all_to_all(outgoing, 'ep', split_axis=1, concat_axis=1, tiled=True)  51.2 us
    all_to_all x2, waiting for transfers between devices, expert_work(): return lax.all_to_all(result, 'ep', split_axis=1, concat_axis=1, tiled=True)  20.6 us
    dot_general x2, matrix products, expert_work(): jnp.einsum('lrf,lfd->lrd', lax.all_gather(activation, 'tp', axis=2, tiled...  10.4 us
    all_to_all x2, starting transfers between devices, expert_work(): return lax.all_to_all(result, 'ep', split_axis=1, concat_axis=1, tiled=True)  9.23 us
    dot_general x2, matrix products, expert_work(): jnp.einsum('lrd,ldf->lrf', shard_piece, gate_weight, preferred_element_ty...  8.95 us
    dot_general x2, matrix products, expert_work(): jnp.einsum('lrd,ldf->lrf', shard_piece, up_weight, preferred_element_type...  5.99 us
  transfers between devices with their start and end apart: 6, of which 5 were waited for; matrix products, arithmetic and copies ran while one was open for 10% of the time, Pallas kernels for 0%

commit v1 on v0

--- a/solution.py
+++ b/solution.py
@@ -1,6 +1,9 @@
+import functools
 import jax
 import jax.numpy as jnp
 from jax import lax
+from jax.experimental import pallas as pl
+from jax.experimental.pallas import tpu as pltpu
 from jax.sharding import PartitionSpec as P
 
 swiglu_limit = 7.0
@@ -87,9 +90,398 @@
     return jnp.sum(picked * route_weights[:, :, None], axis=1).astype(jnp.bfloat16)
 
 
+def layer_kernel(
+    capacity,
+    normed_ref,
+    meta_ref,
+    gate_hbm,
+    up_hbm,
+    down_hbm,
+    out_ref,
+    gate_w,
+    up_w,
+    down_w,
+    toks,
+    meta_in,
+    rows,
+    acts,
+    weighted,
+    pair_out,
+    pair_in,
+    back_out,
+    back_in,
+    total_ref,
+    weight_sem,
+    local_sem,
+    meta_send,
+    meta_recv,
+    line_send,
+    line_recv,
+    side_send,
+    side_recv,
+    pair_send,
+    pair_recv,
+    act_send,
+    act_recv,
+    sum_send,
+    sum_recv,
+    back_send,
+    back_recv,
+):
+    sources = meta_ref.shape[0]
+    chips = sources // 2
+    local_count = gate_w.shape[0]
+    units = gate_w.shape[2]
+    tok_rows = normed_ref.shape[1]
+    me = lax.axis_index("ep")
+    tp = lax.axis_index("tp")
+    z, core = me // 2, me % 2
+    y, x = tp // 2, tp % 2
+    tp_x = y * 2 + (1 - x)
+    tp_y = (1 - y) * 2 + x
+    tp_xy = (1 - y) * 2 + (1 - x)
+    mate = z * 2 + (1 - core)
+
+    def partner(k):
+        other, bit, left = 0 * z, 1, z
+        while bit < chips:
+            digit = left % 2
+            other = other + bit * ((1 - digit) if k & bit else digit)
+            left, bit = left // 2, bit * 2
+        return other
+
+    def place(ep, column):
+        return {"ep": ep, "tp": column}
+
+    def remote(source, target, send, recv, where):
+        return pltpu.make_async_remote_copy(
+            src_ref=source,
+            dst_ref=target,
+            send_sem=send,
+            recv_sem=recv,
+            device_id=where,
+            device_id_type=pl.DeviceIdType.MESH,
+        )
+
+    loads = []
+    for n, (hbm, vmem) in enumerate(((gate_hbm, gate_w), (up_hbm, up_w), (down_hbm, down_w))):
+        loads.append(pltpu.make_async_copy(hbm, vmem, weight_sem.at[n]))
+        loads[-1].start()
+    own_tok = pltpu.make_async_copy(normed_ref, toks.at[me], local_sem.at[0])
+    own_tok.start()
+    own_meta = pltpu.make_async_copy(meta_ref.at[me], meta_in.at[me], local_sem.at[1])
+    own_meta.start()
+
+    barrier = pltpu.get_barrier_semaphore()
+    for d in range(1, sources):
+        pl.semaphore_signal(
+            barrier, inc=1, device_id=place((me + d) % sources, tp), device_id_type=pl.DeviceIdType.MESH
+        )
+    for column in (tp_x, tp_y):
+        pl.semaphore_signal(
+            barrier, inc=1, device_id=place(me, column), device_id_type=pl.DeviceIdType.MESH
+        )
+    pl.semaphore_wait(barrier, sources + 1)
+
+    pending = []
+
+    def go(copy):
+        copy.start()
+        pending.append(copy)
+        return copy
+
+    metas = [
+        go(
+            remote(
+                meta_ref.at[(me + d) % sources],
+                meta_in.at[me],
+                meta_send.at[d],
+                meta_recv.at[d],
+                place((me + d) % sources, tp),
+            )
+        )
+        for d in range(1, sources)
+    ]
+    own_pair = go(
+        remote(normed_ref, toks.at[me], pair_send.at[0], pair_recv.at[0], place(mate, tp))
+    )
+    lines = {
+        k: go(
+            remote(
+                normed_ref.at[x],
+                toks.at[me, x],
+                line_send.at[k],
+                line_recv.at[k],
+                place(partner(k) * 2 + core, tp),
+            )
+        )
+        for k in range(1, chips)
+    }
+
+    pairs, sides, half_pairs = {}, {}, {}
+
+    def spread_line(k):
+        src = partner(k) * 2 + core
+        lines[k].wait_recv()
+        piece = toks.at[src, x]
+        sides[k] = go(remote(piece, piece, side_send.at[k], side_recv.at[k], place(me, tp_x)))
+        pairs[k] = go(
+            remote(piece, piece, pair_send.at[2 * k], pair_recv.at[2 * k], place(mate, tp))
+        )
+
+    def spread_side(k):
+        src = partner(k) * 2 + core
+        sides[k].wait_recv()
+        piece = toks.at[src, 1 - x]
+        half_pairs[k] = go(
+            remote(piece, piece, pair_send.at[2 * k + 1], pair_recv.at[2 * k + 1], place(mate, tp))
+        )
+        pairs[k].wait_recv()
+        half_pairs[k].wait_recv()
+
+    def chosen(source):
+        slots = meta_in[source]
+        at = lax.broadcasted_iota(jnp.int32, (capacity, tok_rows), 0).astype(jnp.float32)
+        hits = [at == slots[n : n + 1, :] for n in range(local_count)]
+        ones = jnp.concatenate([h.astype(jnp.float32) for h in hits], axis=0)
+        scale = jnp.concatenate(
+            [
+                jnp.sum(
+                    jnp.where(hits[n], slots[local_count + n : local_count + n + 1, :], 0.0),
+                    axis=1,
+                    keepdims=True,
+                )
+                for n in range(local_count)
+            ],
+            axis=0,
+        )
+        return ones.astype(jnp.bfloat16), scale
+
+    halves = toks.shape[1]
+    width = toks.shape[3]
+
+    def first_half(k):
+        s = partner(k)
+
+        @pl.loop(0, 2)
+        def _(j):
+            ones, _ = chosen(2 * s + j)
+            for h in range(halves):
+                got = jnp.dot(ones, toks[2 * s + j, h], preferred_element_type=jnp.float32)
+                got = got.astype(jnp.bfloat16)
+                for n in range(local_count):
+                    rows[n, j, :, h * width : (h + 1) * width] = got[
+                        n * capacity : (n + 1) * capacity
+                    ]
+
+        @pl.loop(0, local_count)
+        def _(n):
+            block = rows[n].reshape(2 * capacity, halves * width)
+            cut = units // 2
+            for part in range(2):
+                cols = slice(part * cut, (part + 1) * cut)
+                gate = jnp.dot(block, gate_w[n, :, cols], preferred_element_type=jnp.float32)
+                up = jnp.dot(block, up_w[n, :, cols], preferred_element_type=jnp.float32)
+                acts[k, tp, n, :, cols] = clamped_units(gate, up).astype(jnp.bfloat16)
+
+    own_x, own_y, fwd_y = {}, {}, {}
+
+    def send_act(k):
+        piece = acts.at[k, tp]
+        own_x[k] = go(
+            remote(piece, piece, act_send.at[k, 0], act_recv.at[k, 0], place(me, tp_x))
+        )
+        own_y[k] = go(
+            remote(piece, piece, act_send.at[k, 1], act_recv.at[k, 1], place(me, tp_y))
+        )
+
+    def forward_act(k):
+        own_x[k].wait_recv()
+        piece = acts.at[k, tp_x]
+        fwd_y[k] = go(
+            remote(piece, piece, act_send.at[k, 2], act_recv.at[k, 2], place(me, tp_y))
+        )
+
+    sums = {}
+
+    def second_half(k):
+        s = partner(k)
+        own_y[k].wait_recv()
+        fwd_y[k].wait_recv()
+
+        @pl.loop(0, local_count)
+        def _(n):
+            total = jnp.zeros((2 * capacity, down_w.shape[2]), jnp.float32)
+            for t in range(acts.shape[1]):
+                total = total + jnp.dot(
+                    acts[k, t, n],
+                    down_w[n, t * units : (t + 1) * units, :],
+                    preferred_element_type=jnp.float32,
+                )
+            weighted[n] = total.reshape(2, capacity, down_w.shape[2])
+
+        def combined(j):
+            ones, scale = chosen(2 * s + j)
+            value = jnp.concatenate([weighted[n, j] for n in range(local_count)], axis=0)
+            value = (value * scale).astype(jnp.bfloat16)
+            return lax.dot_general(
+                ones, value, (((0,), (0,)), ((), ())), preferred_element_type=jnp.float32
+            )
+
+        pair_out[k] = combined(1 - core).astype(jnp.bfloat16)
+        sums[k] = go(
+            remote(pair_out.at[k], pair_in.at[k], sum_send.at[k], sum_recv.at[k], place(mate, tp))
+        )
+        mine = combined(core)
+        sums[k].wait_recv()
+        both = mine + pair_in[k].astype(jnp.float32)
+        if k == 0:
+            total_ref[...] = both
+        else:
+            back_out[k] = both.astype(jnp.bfloat16)
+            backs[k] = go(
+                remote(
+                    back_out.at[k],
+                    back_in.at[k],
+                    back_send.at[k],
+                    back_recv.at[k],
+                    place(s * 2 + core, tp),
+                )
+            )
+
+    backs = {}
+
+    own_meta.wait()
+    for copy in metas:
+        copy.wait_recv()
+    own_tok.wait()
+    own_pair.wait_recv()
+    loads[0].wait()
+    loads[1].wait()
+    first_half(0)
+    send_act(0)
+    loads[2].wait()
+    for k in range(1, chips):
+        spread_line(k)
+        forward_act(k - 1)
+        spread_side(k)
+        first_half(k)
+        send_act(k)
+        if k >= 2:
+            second_half(k - 2)
+    forward_act(chips - 1)
+    for k in range(max(chips - 2, 0), chips):
+        second_half(k)
+    result = total_ref[...]
+    for k in range(1, chips):
+        backs[k].wait_recv()
+        result = result + back_in[k].astype(jnp.float32)
+    out_ref[...] = result.astype(out_ref.dtype)
+    for copy in pending:
+        copy.wait_send()
+
+
+def fused_per_device(tokens, norm_gain, route_ids, route_weights, w_gate, w_up, w_down):
+    local_count, width, units = w_gate.shape
+    out_cols = w_down.shape[2]
+    sources = lax.axis_size("ep")
+    tp_count = lax.axis_size("tp")
+    experts = local_count * sources
+    tok_rows, top_count = route_ids.shape
+    capacity = 3 * tok_rows * top_count // (2 * experts)
+    chips = sources // 2
+    half = width // 2
+    values = tokens.astype(jnp.float32)
+    row_mean = jnp.mean(values, axis=1, keepdims=True)
+    centred = values - row_mean
+    row_var = jnp.mean(centred * centred, axis=1, keepdims=True)
+    normed = (centred * lax.rsqrt(row_var + norm_eps) * norm_gain).astype(jnp.bfloat16)
+    normed = jnp.stack([normed[:, :half], normed[:, half:]], axis=0)
+    hits = route_ids[:, :, None] == jnp.arange(experts, dtype=jnp.int32)[None, None, :]
+    named = jnp.any(hits, axis=1)
+    weight_of = jnp.sum(jnp.where(hits, route_weights[:, :, None], 0.0), axis=1)
+    order = jnp.arange(tok_rows)
+    before = (order[:, None] > order[None, :]).astype(jnp.bfloat16)
+    slot = jnp.dot(before, named.astype(jnp.bfloat16), preferred_element_type=jnp.float32)
+    slot = jnp.where(named, slot, -1.0)
+    pad = (-2 * local_count) % 8
+    meta = jnp.concatenate(
+        [
+            slot.T.reshape(sources, local_count, tok_rows),
+            weight_of.T.reshape(sources, local_count, tok_rows),
+            jnp.zeros((sources, pad, tok_rows), jnp.float32),
+        ],
+        axis=1,
+    )
+    dma = pltpu.SemaphoreType.DMA
+    bf16 = jnp.bfloat16
+    vmem = pl.BlockSpec(memory_space=pltpu.VMEM)
+    hbm = pl.BlockSpec(memory_space=pltpu.HBM)
+    return pl.pallas_call(
+        functools.partial(layer_kernel, capacity),
+        out_shape=jax.ShapeDtypeStruct((tok_rows, out_cols), bf16),
+        in_specs=[vmem, vmem, hbm, hbm, hbm],
+        out_specs=vmem,
+        scratch_shapes=[
+            pltpu.VMEM(w_gate.shape, bf16),
+            pltpu.VMEM(w_up.shape, bf16),
+            pltpu.VMEM(w_down.shape, bf16),
+            pltpu.VMEM((sources, 2, tok_rows, half), bf16),
+            pltpu.VMEM(meta.shape, jnp.float32),
+            pltpu.VMEM((local_count, 2, capacity, width), bf16),
+            pltpu.VMEM((chips, tp_count, local_count, 2 * capacity, units), bf16),
+            pltpu.VMEM((local_count, 2, capacity, out_cols), jnp.float32),
+            pltpu.VMEM((chips, tok_rows, out_cols), bf16),
+            pltpu.VMEM((chips, tok_rows, out_cols), bf16),
+            pltpu.VMEM((chips, tok_rows, out_cols), bf16),
+            pltpu.VMEM((chips, tok_rows, out_cols), bf16),
+            pltpu.VMEM((tok_rows, out_cols), jnp.float32),
+            dma((3,)),
+            dma((2,)),
+            dma((sources,)),
+            dma((sources,)),
+            dma((chips,)),
+            dma((chips,)),
+            dma((chips,)),
+            dma((chips,)),
+            dma((2 * chips,)),
+            dma((2 * chips,)),
+            dma((chips, 3)),
+            dma((chips, 3)),
+            dma((chips,)),
+            dma((chips,)),
+            dma((chips,)),
+            dma((chips,)),
+        ],
+        compiler_params=pltpu.CompilerParams(
+            collective_id=0, has_side_effects=True, vmem_limit_bytes=60 * 1024 * 1024
+        ),
+    )(normed, meta, w_gate, w_up, w_down)
+
+
+def pick_plan(mesh):
+    sources, tp_count = mesh.shape["ep"], mesh.shape["tp"]
+
+    def body(tokens, norm_gain, route_ids, route_weights, w_gate, w_up, w_down):
+        tok_rows, top_count = route_ids.shape
+        experts = w_gate.shape[0] * sources
+        capacity = 3 * tok_rows * top_count // (2 * experts)
+        gathered = 2 * tokens.size * sources + 6 * w_gate.size
+        fused = (
+            tp_count == 4
+            and sources in (4, 8)
+            and capacity % 16 == 0
+            and gathered < 32 * 1024 * 1024
+        )
+        run = fused_per_device if fused else per_device
+        return run(tokens, norm_gain, route_ids, route_weights, w_gate, w_up, w_down)
+
+    return body
+
+
 def solution(mesh):
     return jax.shard_map(
-        per_device,
+        pick_plan(mesh),
         mesh=mesh,
         in_specs=(
             P("ep", None),

time: 270 us -> 141 us (0.52)
  waiting for transfers between devices: 150 us -> 0 us
  Pallas kernels: 0 us -> 133 us
  blocking collectives: 51.2 us -> 0 us
  matrix products: 27 us -> 0.16 us
  between operations: 13.3 us -> 0.11 us
  starting transfers between devices: 9.36 us -> 0 us
  local copies, waits for them, and re-layouts: 8.03 us -> 1.9 us
  other arithmetic: 10 us -> 5.39 us
    pallas_call x0 -> x1, Pallas kernels: none -> 133 us  [fused_per_device(): pl.pallas_call(functools.partial(layer_kernel, capacity), out_shape=jax.S...]
    all_gather x4 -> x0, waiting for transfers between devices: 130 us -> none  [the longest x2 73.4 us: expert_work(): lax.all_gather(activation, 'tp', axis=2, tiled=True)]
    all_to_all x2 -> x0, blocking collectives: 51.2 us -> none  [expert_work(): lax.all_to_all(outgoing, 'ep', split_axis=1, concat_axis=1, tiled=True)]
    dot_general x7 -> x1, matrix products: 27 us -> 0.16 us  [fused_per_device(): jnp.dot(before, named.astype(jnp.bfloat16), preferred_element_type=jnp.fl...]
    all_to_all x2 -> x0, waiting for transfers between devices: 20.6 us -> none  [expert_work(): return lax.all_to_all(result, 'ep', split_axis=1, concat_axis=1, tiled=True)]
    all_to_all x2 -> x0, starting transfers between devices: 9.23 us -> none  [expert_work(): return lax.all_to_all(result, 'ep', split_axis=1, concat_axis=1, tiled=True)]
    gather x1 -> x0, local copies, waits for them, and re-layouts: 3.97 us -> none  [per_device(): flat_out[position].reshape(tok_rows, top_count, columns).astype(jnp.float32)]
    another operation x3 -> x1, other arithmetic: 4.64 us -> 1.08 us  [fused_per_device(): normed = jnp.stack([normed[:, :half], normed[:, half:]], axis=0)]
  transfers between devices with their start and end apart: 6 -> 0, of which waited for: 5 -> 0; matrix products, arithmetic and copies ran while one was open for 10% -> 0% of each run, Pallas kernels for 0% -> 0%
where the time goes in v1:
time: 141 us
  Pallas kernels  133 us (94%)
  other arithmetic  5.39 us (4%)
  local copies, waits for them, and re-layouts  1.9 us (1%)
    pallas_call x1, Pallas kernels, fused_per_device(): pl.pallas_call(functools.partial(layer_kernel, capacity), out_shape=jax.S...  133 us

profile of v1, /device:TPU:0, one launch (start us, length us, event | category | flops | bytes accessed | tf_op | source)
XLA Modules:
  0.0 140.7 jit_solution(7401493376358223633)
XLA Ops:
  0.0 0.0 copy-start
  0.0 0.0 copy-start.2
  0.0 1.5 %convert_reduce_fusion = f32[256]{0:T(256)S(1)} fusion(bf16[256,2048]{1,0:T(8,128)(2,1)} %param.7), kind=kLoop, calls=%fused_computation.1 | loop fusion | flops 1048320 | bytes 1049600 | tf_op jit(solution)/shard_map/reduce_sum | solution.py:395
  1.5 1.6 %fusion.2 = f32[256]{0:T(256)S(1)} fusion(bf16[256,2048]{1,0:T(8,128)(2,1)} %param.7, f32[256]{0:T(256)S(1)} %broadcast_multiply_fusion), kind=kLoop, calls=%fused_computation.4 | loop fusion | flops 2096896 | bytes 1050624 | tf_op jit(solution)/shard_map/reduce_sum | solution.py:397
  3.2 0.0 copy-done
  3.2 0.0 copy-done.2
  3.2 0.4 fusion.4
  3.6 0.0 copy-start.1
  3.6 0.0 copy-start.3
  3.6 0.1 slice_bitcast_fusion.1
  3.7 1.1 pad_maximum_fusion.normed_ref
  4.8 0.0 copy-done.1
  4.8 0.2 convolution_select_fusion
  5.0 0.0 copy-done.3
  5.1 0.1 pad.2.clone
  5.2 0.7 maximum_maximum_fusion.meta_ref
  5.9 133.1 %shard_map.73 = bf16[256,512]{1,0:T(8,128)(2,1)} custom-call(bf16[2,256,1024]{2,1,0:T(8,128)(2,1)} %pad_maximum_fusion.normed_ref, f32[8,8,256]{2,1,0:T(8,128)} %maximum_maximum_fusion.meta_ref, bf16[2,2048,512]{2,1,0:T(8,128)(2,1)} %gate_hbm.1, bf16[2,2048,512]{2,1,0:T(8,128)(2,1)} %up_hbm.1, bf16[2,2048,512]{2,1,0:T(8,128)(2,1)} %down_hbm.1), custom_call_target="tpu_custom_call" | custom-call | tf_op jit(solution)/shard_map/pallas_call | solution.py:420
  139.0 1.7 %copy.11 = bf16[256,512]{1,0:T(8,128)(2,1)} copy(bf16[256,512]{1,0:T(8,128)(2,1)} %shard_map.73) | data formatting | bytes 524288
  (7 shorter events, 0.1 us)
Async XLA Ops:
  0.0 3.2 %copy-start = (bf16[256,2048]{1,0:T(8,128)(2,1)S(1)}, bf16[256,2048]{1,0:T(8,128)(2,1)}, u32[]{:S(2)}) copy-start(bf16[256,2048]{1,0:T(8,128)(2,1)} %param.7) | copy-start | bytes 3145732
  0.0 3.2 %copy-start.2 = (f32[2048]{0:T(1024)S(1)}, f32[2048]{0:T(1024)}, u32[]{:S(2)}) copy-start(f32[2048]{0:T(1024)} %param.8) | copy-start | bytes 24580
  3.6 1.2 copy-start.1
  3.6 1.4 %copy-start.3 = (f32[256,4]{0,1:T(4,128)S(1)}, f32[256,4]{0,1:T(4,128)}, u32[]{:S(2)}) copy-start(f32[256,4]{0,1:T(4,128)} %param.10) | copy-start | bytes 12292

commit v2 on v1

--- a/solution.py
+++ b/solution.py
@@ -141,14 +141,15 @@
     tp_y = (1 - y) * 2 + x
     tp_xy = (1 - y) * 2 + (1 - x)
     mate = z * 2 + (1 - core)
+    own_half = (x + y) % 2
 
     def partner(k):
-        other, bit, left = 0 * z, 1, z
-        while bit < chips:
-            digit = left % 2
-            other = other + bit * ((1 - digit) if k & bit else digit)
-            left, bit = left // 2, bit * 2
-        return other
+        chosen_chip = 0 * z
+        for at in range(chips):
+            order = sorted(range(chips), key=lambda c: (abs(c - at), c))
+            gap = (z - at) * (z - at)
+            chosen_chip = chosen_chip + order[k] * (1 - (gap + chips * chips - 1) // (chips * chips))
+        return chosen_chip
 
     def place(ep, column):
         return {"ep": ep, "tp": column}
@@ -205,37 +206,65 @@
     own_pair = go(
         remote(normed_ref, toks.at[me], pair_send.at[0], pair_recv.at[0], place(mate, tp))
     )
-    lines = {
-        k: go(
-            remote(
-                normed_ref.at[x],
-                toks.at[me, x],
-                line_send.at[k],
-                line_recv.at[k],
-                place(partner(k) * 2 + core, tp),
+    def line(chip, up, distance):
+        piece = toks.at[chip * 2 + core, own_half]
+        return remote(
+            normed_ref.at[own_half] if distance is None else piece,
+            piece,
+            line_send.at[up, chip],
+            line_recv.at[up, chip],
+            place((z + 2 * up - 1) * 2 + core, tp),
+        )
+
+    @pl.when(z < chips - 1)
+    def _():
+        line(z, 1, None).start()
+
+    @pl.when(z > 0)
+    def _():
+        line(z, 0, None).start()
+
+    def upward(chip):
+        return (chips + z - chip - 1) // chips
+
+    def goes_on(chip):
+        ahead = z + 2 * upward(chip) - 1
+        return jnp.logical_and(ahead >= 0, ahead < chips)
+
+    pairs, sides, half_pairs = {}, {}, {}
+    cut_rows = tok_rows // 2
+
+    def spread_line(k):
+        chip = partner(k)
+        src = chip * 2 + core
+        up = upward(chip)
+        line(chip, up, k).wait_recv()
+
+        @pl.when(goes_on(chip))
+        def _():
+            line(chip, up, k).start()
+
+        sides[k] = []
+        for n, column in enumerate((tp_x, tp_y)):
+            part = toks.at[src, own_half, pl.ds(n * cut_rows, cut_rows)]
+            sides[k].append(
+                go(remote(part, part, side_send.at[k, n], side_recv.at[k, n], place(me, column)))
             )
-        )
-        for k in range(1, chips)
-    }
-
-    pairs, sides, half_pairs = {}, {}, {}
-
-    def spread_line(k):
-        src = partner(k) * 2 + core
-        lines[k].wait_recv()
-        piece = toks.at[src, x]
-        sides[k] = go(remote(piece, piece, side_send.at[k], side_recv.at[k], place(me, tp_x)))
+        piece = toks.at[src, own_half]
         pairs[k] = go(
             remote(piece, piece, pair_send.at[2 * k], pair_recv.at[2 * k], place(mate, tp))
         )
 
     def spread_side(k):
         src = partner(k) * 2 + core
-        sides[k].wait_recv()
-        piece = toks.at[src, 1 - x]
+        for copy in sides[k]:
+            copy.wait_recv()
+        piece = toks.at[src, 1 - own_half]
         half_pairs[k] = go(
             remote(piece, piece, pair_send.at[2 * k + 1], pair_recv.at[2 * k + 1], place(mate, tp))
         )
+
+    def settle(k):
         pairs[k].wait_recv()
         half_pairs[k].wait_recv()
 
@@ -284,7 +313,7 @@
                 up = jnp.dot(block, up_w[n, :, cols], preferred_element_type=jnp.float32)
                 acts[k, tp, n, :, cols] = clamped_units(gate, up).astype(jnp.bfloat16)
 
-    own_x, own_y, fwd_y = {}, {}, {}
+    own_x, own_y, fwd_y, fwd_x = {}, {}, {}, {}
 
     def send_act(k):
         piece = acts.at[k, tp]
@@ -296,18 +325,24 @@
         )
 
     def forward_act(k):
+        mid = local_count // 2
         own_x[k].wait_recv()
-        piece = acts.at[k, tp_x]
+        piece = acts.at[k, tp_x, pl.ds(0, mid)]
         fwd_y[k] = go(
             remote(piece, piece, act_send.at[k, 2], act_recv.at[k, 2], place(me, tp_y))
         )
+        own_y[k].wait_recv()
+        piece = acts.at[k, tp_y, pl.ds(mid, local_count - mid)]
+        fwd_x[k] = go(
+            remote(piece, piece, act_send.at[k, 3], act_recv.at[k, 3], place(me, tp_x))
+        )
 
     sums = {}
 
     def second_half(k):
         s = partner(k)
-        own_y[k].wait_recv()
         fwd_y[k].wait_recv()
+        fwd_x[k].wait_recv()
 
         @pl.loop(0, local_count)
         def _(n):
@@ -339,17 +374,16 @@
             total_ref[...] = both
         else:
             back_out[k] = both.astype(jnp.bfloat16)
-            backs[k] = go(
+            go(
                 remote(
                     back_out.at[k],
-                    back_in.at[k],
+                    back_in.at[z],
                     back_send.at[k],
-                    back_recv.at[k],
+                    back_recv.at[z],
                     place(s * 2 + core, tp),
                 )
             )
 
-    backs = {}
 
     own_meta.wait()
     for copy in metas:
@@ -361,24 +395,45 @@
     first_half(0)
     send_act(0)
     loads[2].wait()
+    spread_line(1)
+    forward_act(0)
+    if chips > 2:
+        spread_line(2)
     for k in range(1, chips):
-        spread_line(k)
-        forward_act(k - 1)
         spread_side(k)
+        if k + 2 < chips:
+            spread_line(k + 2)
+        settle(k)
         first_half(k)
         send_act(k)
-        if k >= 2:
-            second_half(k - 2)
-    forward_act(chips - 1)
-    for k in range(max(chips - 2, 0), chips):
-        second_half(k)
+        second_half(k - 1)
+        forward_act(k)
+    second_half(chips - 1)
     result = total_ref[...]
     for k in range(1, chips):
-        backs[k].wait_recv()
-        result = result + back_in[k].astype(jnp.float32)
+        other = (z + k) % chips
+        remote(
+            back_out.at[k], back_in.at[other], back_send.at[k], back_recv.at[other], place(mate, tp)
+        ).wait_recv()
+        result = result + back_in[other].astype(jnp.float32)
     out_ref[...] = result.astype(out_ref.dtype)
     for copy in pending:
         copy.wait_send()
+
+    @pl.when(z < chips - 1)
+    def _():
+        line(z, 1, None).wait_send()
+
+    @pl.when(z > 0)
+    def _():
+        line(z, 0, None).wait_send()
+
+    for k in range(1, chips):
+        chip = partner(k)
+
+        @pl.when(goes_on(chip))
+        def _():
+            line(chip, upward(chip), k).wait_send()
 
 
 def fused_per_device(tokens, norm_gain, route_ids, route_weights, w_gate, w_up, w_down):
@@ -440,14 +495,14 @@
             dma((2,)),
             dma((sources,)),
             dma((sources,)),
-            dma((chips,)),
-            dma((chips,)),
-            dma((chips,)),
-            dma((chips,)),
+            dma((2, chips)),
+            dma((2, chips)),
+            dma((chips, 2)),
+            dma((chips, 2)),
             dma((2 * chips,)),
             dma((2 * chips,)),
-            dma((chips, 3)),
-            dma((chips, 3)),
+            dma((chips, 4)),
+            dma((chips, 4)),
             dma((chips,)),
             dma((chips,)),
             dma((chips,)),
@@ -471,6 +526,8 @@
             tp_count == 4
             and sources in (4, 8)
             and capacity % 16 == 0
+            and w_gate.shape[0] % 2 == 0
+            and tok_rows % 32 == 0
             and gathered < 32 * 1024 * 1024
         )
         run = fused_per_device if fused else per_device

time: 141 us -> 114 us (0.81)
  Pallas kernels: 133 us -> 107 us
    pallas_call x1, Pallas kernels: 133 us -> 107 us  [fused_per_device(): pl.pallas_call(functools.partial(layer_kernel, capacity), out_shape=jax.S...]
where the time goes in v2:
time: 114 us
  Pallas kernels  107 us (94%)
  other arithmetic  5.39 us (5%)
  local copies, waits for them, and re-layouts  1.9 us (2%)
    pallas_call x1, Pallas kernels, fused_per_device(): pl.pallas_call(functools.partial(layer_kernel, capacity), out_shape=jax.S...  107 us

profile of v2, /device:TPU:0, one launch (start us, length us, event | category | flops | bytes accessed | tf_op | source)
XLA Modules:
  0.0 114.2 jit_solution(12949812339183060033)
XLA Ops:
  0.0 0.0 copy-start
  0.0 0.0 copy-start.2
  0.0 1.5 %convert_reduce_fusion = f32[256]{0:T(256)S(1)} fusion(bf16[256,2048]{1,0:T(8,128)(2,1)} %param.7), kind=kLoop, calls=%fused_computation.1 | loop fusion | flops 1048320 | bytes 1049600 | tf_op jit(solution)/shard_map/reduce_sum | solution.py:450
  1.5 1.6 %fusion.2 = f32[256]{0:T(256)S(1)} fusion(bf16[256,2048]{1,0:T(8,128)(2,1)} %param.7, f32[256]{0:T(256)S(1)} %broadcast_multiply_fusion), kind=kLoop, calls=%fused_computation.4 | loop fusion | flops 2096896 | bytes 1050624 | tf_op jit(solution)/shard_map/reduce_sum | solution.py:452
  3.2 0.0 copy-done
  3.2 0.0 copy-done.2
  3.2 0.4 fusion.4
  3.6 0.0 copy-start.1
  3.6 0.0 copy-start.3
  3.6 0.1 slice_bitcast_fusion.1
  3.7 1.1 pad_maximum_fusion.normed_ref
  4.8 0.0 copy-done.1
  4.8 0.2 convolution_select_fusion
  5.0 0.0 copy-done.3
  5.1 0.1 pad.2.clone
  5.2 0.7 maximum_maximum_fusion.meta_ref
  5.9 106.6 %shard_map.73 = bf16[256,512]{1,0:T(8,128)(2,1)} custom-call(bf16[2,256,1024]{2,1,0:T(8,128)(2,1)} %pad_maximum_fusion.normed_ref, f32[8,8,256]{2,1,0:T(8,128)} %maximum_maximum_fusion.meta_ref, bf16[2,2048,512]{2,1,0:T(8,128)(2,1)} %gate_hbm.1, bf16[2,2048,512]{2,1,0:T(8,128)(2,1)} %up_hbm.1, bf16[2,2048,512]{2,1,0:T(8,128)(2,1)} %down_hbm.1), custom_call_target="tpu_custom_call" | custom-call | tf_op jit(solution)/shard_map/pallas_call | solution.py:475
  112.5 1.7 %copy.11 = bf16[256,512]{1,0:T(8,128)(2,1)} copy(bf16[256,512]{1,0:T(8,128)(2,1)} %shard_map.73) | data formatting | bytes 524288
  (7 shorter events, 0.1 us)
Async XLA Ops:
  0.0 3.2 %copy-start = (bf16[256,2048]{1,0:T(8,128)(2,1)S(1)}, bf16[256,2048]{1,0:T(8,128)(2,1)}, u32[]{:S(2)}) copy-start(bf16[256,2048]{1,0:T(8,128)(2,1)} %param.7) | copy-start | bytes 3145732
  0.0 3.2 %copy-start.2 = (f32[2048]{0:T(1024)S(1)}, f32[2048]{0:T(1024)}, u32[]{:S(2)}) copy-start(f32[2048]{0:T(1024)} %param.8) | copy-start | bytes 24580
  3.6 1.2 %copy-start.1 = (s32[256,4]{0,1:T(4,128)S(1)}, s32[256,4]{0,1:T(4,128)}, u32[]{:S(2)}) copy-start(s32[256,4]{0,1:T(4,128)} %param.9) | copy-start | bytes 12292
  3.6 1.4 %copy-start.3 = (f32[256,4]{0,1:T(4,128)S(1)}, f32[256,4]{0,1:T(4,128)}, u32[]{:S(2)}) copy-start(f32[256,4]{0,1:T(4,128)} %param.10) | copy-start | bytes 12292
